TPU v7x, 32 devices: a whole 2x2x4 slice. The times are simulated.
32 devices in a mesh: ep: 8 (over z, y), tp: 4 (over x, core).
Axes of the slice: x: 2, y: 2, z: 4, core: 2. Of those that a mesh axis runs over, the one named last changes fastest.
Arguments:
- hidden: bfloat16 [256, 2048], P('ep')
- norm_gains: float32 [4, 2048], replicated, may hold values from 0.1 to 1.9
- w_query: bfloat16 [2048, 1024], P(None, 'tp'), may hold values from -0.125 to 0.125
- w_key: bfloat16 [2048, 1024], P(None, 'tp'), may hold values from -0.125 to 0.125
- w_value: bfloat16 [2048, 1024], P(None, 'tp'), may hold values from -0.125 to 0.125
- w_outgate: bfloat16 [2048, 1024], P(None, 'tp'), may hold values from -0.125 to 0.125
- w_input_gate: bfloat16 [2048, 8], replicated, may hold values from -0.125 to 0.125
- w_forget_gate: bfloat16 [2048, 8], replicated, may hold values from -0.125 to 0.125
- forget_bias: float32 [8], replicated, may hold values from -1 to 4
- w_mix_out: bfloat16 [1024, 2048], P('tp')
- state_matrix: float32 [256, 8, 128, 128], P('ep', 'tp'), may hold values from -0.6 to 0.6
- state_norm: float32 [256, 8, 128], P('ep', 'tp'), may hold values from -0.6 to 0.6
- state_max: float32 [256, 8], P('ep', 'tp'), may hold values from -4 to 4
- routes: int32 [256, 2], P('ep'), may hold values from 0 to 7, all different within a row; in each aligned block of 32 rows (0 to 31, 32 to 63, ...) at most 16 rows name the same one
- route_scores: float32 [256, 2], P('ep'), may hold values from 0.1 to 1
- expert_gate: bfloat16 [8, 2048, 3584], P('ep', None, 'tp'), may hold values from -0.125 to 0.125
- expert_up: bfloat16 [8, 2048, 3584], P('ep', None, 'tp'), may hold values from -0.125 to 0.125
- expert_down: bfloat16 [8, 3584, 2048], P('ep', 'tp')
- dense_gate: bfloat16 [2048, 5632], P('tp', 'ep'), may hold values from -0.125 to 0.125
- dense_up: bfloat16 [2048, 5632], P('tp', 'ep'), may hold values from -0.125 to 0.125
- dense_down: bfloat16 [5632, 2048], P('ep', 'tp')
- dense_mix: float32 [2048], replicated, may hold values from -0.25 to 0.25
Outputs:
- new_hidden: bfloat16 [256, 2048], P('ep', 'tp')
- new_matrix: float32 [256, 8, 128, 128], P('ep', 'tp')
- new_norm: float32 [256, 8, 128], P('ep', 'tp')
- new_max: float32 [256, 8], P('ep', 'tp')
Inputs may be any that keep to these rules, and one draw needn't show every extreme that they name: `routes`: each row names 2 different experts. Among the rows of one index of ep (an aligned block of 32 rows) no expert is named by more than 16 rows, and in every draw some expert is named by exactly 16 rows of some block.
All inputs are finite; a program needn't handle non-finite values.
Results may differ from a plain program's by a relative error of at most 0.02.
Values may be sent and summed in bfloat16 or wider, within the bound.
No kernel may reach another device: no remote copies, remote signals or barrier semaphores. Data moves between devices by JAX's collectives and lax.ppermute only.
A program may use at most 128 MiB of HBM per device.

v0:
```python
import jax
import jax.numpy as jnp
from jax import lax
from jax.sharding import PartitionSpec as P

EPS = 1e-06


def settle(values):
    return lax.optimization_barrier(values.astype(jnp.bfloat16)).astype(jnp.float32)


def local(
    hidden,
    norm_gains,
    w_query,
    w_key,
    w_value,
    w_outgate,
    w_input_gate,
    w_forget_gate,
    forget_bias,
    w_mix_out,
    state_matrix,
    state_norm,
    state_max,
    routes,
    route_scores,
    expert_gate,
    expert_up,
    expert_down,
    dense_gate,
    dense_up,
    dense_down,
    dense_mix,
):
    tp_count = lax.axis_size("tp")
    ep_count = lax.axis_size("ep")
    tp_place = lax.axis_index("tp")
    seq_local, width = hidden.shape
    heads_local = state_matrix.shape[1]
    head_width = state_matrix.shape[2]
    part_width = width // tp_count
    feature_first = tp_place * part_width
    start_f = hidden.astype(jnp.float32)
    normed_in = (
        start_f
        * lax.rsqrt(jnp.mean(start_f * start_f, axis=-1, keepdims=True) + EPS)
        * norm_gains[0]
    ).astype(jnp.bfloat16)
    query_f = jnp.dot(normed_in, w_query, preferred_element_type=jnp.float32)
    key_f = jnp.dot(normed_in, w_key, preferred_element_type=jnp.float32)
    value_f = jnp.dot(normed_in, w_value, preferred_element_type=jnp.float32)
    gate_f = jnp.dot(normed_in, w_outgate, preferred_element_type=jnp.float32)
    head_first = tp_place * heads_local
    input_weight = lax.dynamic_slice_in_dim(w_input_gate, head_first, heads_local, 1)
    forget_weight = lax.dynamic_slice_in_dim(w_forget_gate, head_first, heads_local, 1)
    forget_local = lax.dynamic_slice_in_dim(forget_bias, head_first, heads_local, 0)
    in_gate = jnp.dot(normed_in, input_weight, preferred_element_type=jnp.float32)
    log_forget = jax.nn.log_sigmoid(
        jnp.dot(normed_in, forget_weight, preferred_element_type=jnp.float32) + forget_local
    )
    query = settle(query_f).reshape(seq_local, heads_local, head_width)
    keys = settle(key_f).reshape(seq_local, heads_local, head_width) * head_width ** (-0.5)
    values = settle(value_f).reshape(seq_local, heads_local, head_width)
    carried = log_forget + state_max
    new_max = jnp.maximum(carried, in_gate)
    keep = jnp.exp(carried - new_max)
    write = jnp.exp(in_gate - new_max)
    written = write[:, :, None] * keys
    new_matrix = (
        keep[:, :, None, None] * state_matrix + written[:, :, :, None] * values[:, :, None, :]
    )
    new_norm = keep[:, :, None] * state_norm + written
    numer = jnp.einsum("shd,shdv->shv", query, new_matrix)
    denom = jnp.einsum("shd,shd->sh", query, new_norm)
    read = numer / jnp.maximum(jnp.abs(denom), jnp.exp(-new_max))[:, :, None]
    mixed = (
        jax.nn.sigmoid(settle(gate_f)) * read.reshape(seq_local, heads_local * head_width)
    ).astype(jnp.bfloat16)
    branch_terms = settle(jnp.dot(mixed, w_mix_out, preferred_element_type=jnp.float32))
    branch = settle(
        lax.psum_scatter(
            branch_terms.astype(jnp.bfloat16), "tp", scatter_dimension=1, tiled=True
        ).astype(jnp.float32)
    )
    start_part = lax.dynamic_slice_in_dim(start_f, feature_first, part_width, 1)
    gain_rows = lax.dynamic_slice_in_dim(norm_gains, feature_first, part_width, 1)
    lifted = gain_rows[1] * branch
    mix_weight = gain_rows[2] * lax.dynamic_slice_in_dim(dense_mix, feature_first, part_width, 0)
    branch_sq, start_sq, cross_sum, lifted_sq, start_dot, lifted_dot = lax.psum(
        (
            jnp.sum(branch * branch, axis=-1),
            jnp.sum(start_part * start_part, axis=-1),
            jnp.sum(start_part * lifted, axis=-1),
            jnp.sum(lifted * lifted, axis=-1),
            jnp.sum(start_part * mix_weight, axis=-1),
            jnp.sum(lifted * mix_weight, axis=-1),
        ),
        "tp",
    )
    branch_scale = lax.rsqrt(branch_sq / width + EPS)
    residual_f = start_part + lifted * branch_scale[:, None]
    resid_sq = start_sq + 2.0 * branch_scale * cross_sum + branch_scale * branch_scale * lifted_sq
    gate_dot = start_dot + branch_scale * lifted_dot
    scale_two = lax.rsqrt(resid_sq / width + EPS)
    mix_gate = jax.nn.sigmoid(scale_two * gate_dot)
    residual = settle(residual_f)
    normed = (residual_f * scale_two[:, None] * gain_rows[2]).astype(jnp.bfloat16)
    rows_in = lax.all_gather(normed, "ep", axis=0, tiled=True)
    dense_pre = jnp.concatenate(
        [
            jnp.dot(rows_in, dense_gate, preferred_element_type=jnp.float32),
            jnp.dot(rows_in, dense_up, preferred_element_type=jnp.float32),
        ],
        axis=1,
    )
    dense_pre = lax.psum(dense_pre.astype(jnp.bfloat16), "tp").astype(jnp.float32)
    dense_pre_gate, dense_pre_up = jnp.split(dense_pre, 2, axis=1)
    dense_hidden = (jax.nn.silu(dense_pre_gate) * dense_pre_up).astype(jnp.bfloat16)
    dense_out = lax.psum_scatter(
        jnp.dot(dense_hidden, dense_down, preferred_element_type=jnp.float32).astype(jnp.bfloat16),
        "ep",
        scatter_dimension=0,
        tiled=True,
    ).astype(jnp.float32)
    route_width = routes.shape[1]
    expert_count = ep_count * expert_gate.shape[0]
    capacity = 2 * seq_local * route_width // ep_count
    flat_expert = routes.reshape(-1)
    picks = (flat_expert[:, None] == jnp.arange(expert_count, dtype=jnp.int32)[None, :]).astype(
        jnp.int32
    )
    ranks = jnp.sum(jnp.cumsum(picks, axis=0) * picks, axis=1) - 1
    slot_index = flat_expert * capacity + ranks
    placing = (
        jnp.arange(expert_count * capacity, dtype=jnp.int32)[:, None] == slot_index[None, :]
    ).astype(jnp.bfloat16)
    repeated = jnp.repeat(normed, route_width, axis=0)
    outgoing = (
        jnp.dot(placing, repeated, preferred_element_type=jnp.float32)
        .astype(jnp.bfloat16)
        .reshape(expert_count, capacity, part_width)
    )
    arrived = lax.all_to_all(outgoing, "ep", split_axis=0, concat_axis=0, tiled=True)
    full_rows = lax.all_gather(arrived, "tp", axis=2, tiled=True)
    flat_rows = full_rows.reshape(-1, width)
    gate_pre = jnp.dot(flat_rows, expert_gate[0], preferred_element_type=jnp.float32)
    up_pre = jnp.dot(flat_rows, expert_up[0], preferred_element_type=jnp.float32)
    hidden_units = (jax.nn.silu(gate_pre) * up_pre).astype(jnp.bfloat16)
    partial_out = settle(jnp.dot(hidden_units, expert_down[0], preferred_element_type=jnp.float32))
    summed_out = lax.psum_scatter(
        partial_out.astype(jnp.bfloat16), "tp", scatter_dimension=1, tiled=True
    )
    returned = lax.all_to_all(
        summed_out.reshape(arrived.shape), "ep", split_axis=0, concat_axis=0, tiled=True
    )
    picked = lax.dot_general(
        placing,
        returned.reshape(expert_count * capacity, part_width),
        (((0,), (0,)), ((), ())),
        preferred_element_type=jnp.float32,
    )
    share = route_scores / jnp.sum(route_scores, axis=-1, keepdims=True)
    moe_out = jnp.sum(
        picked.reshape(seq_local, route_width, part_width) * share[:, :, None], axis=1
    )
    ffn = moe_out + mix_gate[:, None] * dense_out
    ffn_sq = lax.psum(jnp.sum(ffn * ffn, axis=-1), "tp")
    new_hidden = (residual + gain_rows[3] * ffn * lax.rsqrt(ffn_sq / width + EPS)[:, None]).astype(
        jnp.bfloat16
    )
    return (new_hidden, new_matrix, new_norm, new_max)


def solution(mesh):
    placed = (
        P("ep", None),
        P(),
        P(None, "tp"),
        P(None, "tp"),
        P(None, "tp"),
        P(None, "tp"),
        P(),
        P(),
        P(),
        P("tp", None),
        P("ep", "tp", None, None),
        P("ep", "tp", None),
        P("ep", "tp"),
        P("ep", None),
        P("ep", None),
        P("ep", None, "tp"),
        P("ep", None, "tp"),
        P("ep", "tp", None),
        P("tp", "ep"),
        P("tp", "ep"),
        P("ep", "tp"),
        P(),
    )
    return jax.shard_map(
        local,
        mesh=mesh,
        in_specs=placed,
        out_specs=(P("ep", "tp"), P("ep", "tp", None, None), P("ep", "tp", None), P("ep", "tp")),
        check_vma=False,
    )
```

profile of v0, /device:TPU:0, one launch (start us, length us, event | category | flops | bytes accessed | tf_op | source)
XLA Modules:
  0.0 237.0 jit_solution(14512095781934341025)
XLA Ops:
  7.3 0.9 slice.14
  8.2 1.0 multiply_reduce_fusion
  9.2 1.6 convolution_convert_fusion.7
  10.9 1.1 fusion.44
  12.8 1.2 subtract_exponential_fusion
  14.1 1.6 convolution_convert_fusion.6
  15.8 1.6 convolution_convert_fusion.5
  18.7 3.7 %multiply_add_fusion = f32[32,2,128,128]{3,2,1,0:T(8,128)S(1)} fusion(f32[32,2,128,128]{3,2,1,0:T(8,128)} %param.32, f32[32,2,128]{2,1,0:T(2,128)S(1)} %reshape.112, f32[32,2,128]{2,1,0:T(2,128)S(1)} %get-tuple-element.20, f32[32,2]{1,0:T(8,128)S(1)} %copy.31), kind=kLoop, calls=%fused_computation | loop fusion | flops 3145728 | bytes 8454400 | tf_op jit(solution)/shard_map/add | solution.py:72
  22.5 2.0 copy-done.1
  25.3 0.9 convolution_convert_fusion
  26.8 0.9 fusion.56
  28.5 20.2 %reduce-scatter.4.cloned.1.call-done = bf16[32,512]{1,0:T(8,128)(2,1)} async-done(((bf16[32,2048]{1,0:T(8,128)(2,1)}), bf16[32,512]{1,0:T(8,128)(2,1)}) %reduce-scatter.4.cloned.1.call-update) | async-done | bytes 32784 | tf_op jit(solution)/shard_map/reduce_scatter | solution.py:83
  48.7 1.0 multiply_reduce_fusion.2
  49.7 5.8 %all-reduce = (f32[32]{0:T(128)S(1)}, f32[32]{0:T(128)S(1)}, f32[32]{0:T(128)S(1)}, f32[32]{0:T(128)S(1)}, f32[32]{0:T(128)S(1)}, /*index=5*/f32[32]{0:T(128)S(1)}) all-reduce(f32[32]{0:T(128)S(1)} %get-tuple-element.9, f32[32]{0:T(128)S(1)} %get-tuple-element.8, f32[32]{0:T(128)S(1)} %get-tuple-element.5, ...), channel_id=1, replica_groups=mesh['ep'=8,'tp'=4] {'tp'}, use_global_device_ids=true, to_apply=%region_3.4 | all-reduce | flops 192 | bytes 1536 | tf_op jit(solution)/shard_map/psum | solution.py:91
  55.5 0.9 multiply_convert_fusion.1
  56.3 31.2 %all_gather.7 = bf16[256,512]{1,0:T(8,128)(2,1)S(1)} all-gather(bf16[32,512]{1,0:T(8,128)(2,1)S(1)} %get-tuple-element.23), channel_id=1, replica_groups=mesh['ep'=8,'tp'=4] {'ep'}, dimensions={0}, use_global_device_ids=true | all-gather | bytes 294912 | tf_op jit(solution)/shard_map/all_gather | solution.py:110
  89.2 5.3 %all-to-all-start = ((bf16[8,16,512]{2,1,0:T(8,128)(2,1)}), bf16[8,16,512]{2,1,0:T(8,128)(2,1)S(1)}, u32[]{:S(2)}, u32[]{:S(2)}) async-start(bf16[8,16,512]{2,1,0:T(8,128)(2,1)} %bitcast.6), calls=%async_computation.1 | async-start | bytes 262144 | tf_op jit(solution)/shard_map/all_to_all | solution.py:145
  94.5 0.9 pad_maximum_fusion
  95.5 6.3 %all-to-all-done = bf16[8,16,512]{2,1,0:T(8,128)(2,1)S(1)} async-done(((bf16[8,16,512]{2,1,0:T(8,128)(2,1)}), bf16[8,16,512]{2,1,0:T(8,128)(2,1)S(1)}, u32[]{:S(2)}, u32[]{:S(2)}) %all-to-all-start) | async-done | bytes 131104 | tf_op jit(solution)/shard_map/all_to_all | solution.py:145
  101.8 9.2 %all_gather.6 = bf16[8,16,2048]{2,1,0:T(8,128)(2,1)S(1)} all-gather(bf16[8,16,512]{2,1,0:T(8,128)(2,1)S(1)} %all-to-all-done), channel_id=1, replica_groups=mesh['ep'=8,'tp'=4] {'tp'}, dimensions={2}, use_global_device_ids=true | all-gather | bytes 655360 | tf_op jit(solution)/shard_map/all_gather | solution.py:146
  111.0 2.8 %fusion.4 = f32[128,896]{1,0:T(8,128)S(1)} fusion(bf16[128,2048]{1,0:T(8,128)(2,1)S(1)} %bitcast.51, bf16[1,2048,896]{2,1,0:T(8,128)(2,1)} %param.37), kind=kOutput, calls=%fused_computation.5 | convolution fusion | flops 469762048 | bytes 4653056 | tf_op jit(solution)/shard_map/dot_general | solution.py:148
  113.9 5.5 %fusion.6 = bf16[128,2048]{1,0:T(8,128)(2,1)} fusion(bf16[1,896,2048]{2,1,0:T(8,128)(2,1)} %param.39, bf16[128,2048]{1,0:T(8,128)(2,1)S(1)} %bitcast.52, bf16[1,2048,896]{2,1,0:T(8,128)(2,1)} %param.38, f32[128,896]{1,0:T(8,128)S(1)} %fusion.4), kind=kOutput, calls=%fused_computation.7 | convolution fusion | flops 940474368 | bytes 8847360 | tf_op jit(solution)/shard_map/dot_general | solution.py:151
  119.4 13.2 %all-reduce.3.cloned.1.call-done = bf16[256,1408]{0,1:T(8,128)(2,1)} async-done(((bf16[256,1408]{0,1:T(8,128)(2,1)}), bf16[256,1408]{0,1:T(8,128)(2,1)}) %all-reduce.3.cloned.1.call-update) | async-done | bytes 720912 | tf_op jit(solution)/shard_map/psum | solution.py:118
  132.6 1.2 convert_element_type.94
  133.8 1.1 convolution_convert_fusion.3
  134.9 21.8 %reduce-scatter.6.cloned.1.call-done = bf16[128,512]{1,0:T(8,128)(2,1)} async-done(((bf16[128,2048]{1,0:T(8,128)(2,1)}), bf16[128,512]{1,0:T(8,128)(2,1)}) %reduce-scatter.6.cloned.1.call-update) | async-done | bytes 131088 | tf_op jit(solution)/shard_map/reduce_scatter | solution.py:152
  156.7 5.5 %all-to-all-start.1 = ((bf16[8,16,512]{2,1,0:T(8,128)(2,1)}), bf16[8,16,512]{2,1,0:T(8,128)(2,1)S(1)}, u32[]{:S(2)}, u32[]{:S(2)}) async-start(bf16[8,16,512]{2,1,0:T(8,128)(2,1)} %bitcast.62), calls=%async_computation.3 | async-start | bytes 262144 | tf_op jit(solution)/shard_map/all_to_all | solution.py:155
  162.4 7.2 %all-to-all-done.1 = bf16[8,16,512]{2,1,0:T(8,128)(2,1)S(1)} async-done(((bf16[8,16,512]{2,1,0:T(8,128)(2,1)}), bf16[8,16,512]{2,1,0:T(8,128)(2,1)S(1)}, u32[]{:S(2)}, u32[]{:S(2)}) %all-to-all-start.1) | async-done | bytes 131104 | tf_op jit(solution)/shard_map/all_to_all | solution.py:155
  169.8 52.6 %reduce-scatter.8.cloned.1.call-done = bf16[32,512]{1,0:T(8,128)(2,1)} async-done(((bf16[256,512]{1,0:T(8,128)(2,1)}), bf16[32,512]{1,0:T(8,128)(2,1)}) %reduce-scatter.8.cloned.1.call-update) | async-done | bytes 32784 | tf_op jit(solution)/shard_map/reduce_scatter | solution.py:121
  222.4 0.9 multiply_reduce_fusion.1
  223.3 5.7 %psum.63 = f32[32]{0:T(128)S(1)} all-reduce(f32[32]{0:T(128)S(1)} %multiply_reduce_fusion.1), channel_id=1, replica_groups=mesh['ep'=8,'tp'=4] {'tp'}, use_global_device_ids=true, to_apply=%region_22.23 | all-reduce | flops 32 | bytes 256 | tf_op jit(solution)/shard_map/psum | solution.py:169
  229.0 1.5 add_convert_fusion
  (65 shorter events, 6.6 us)
Async XLA Ops:
  7.2 18.1 %copy-start = (bf16[256,2048]{1,0:T(8,128)(2,1)S(1)}, bf16[256,2048]{1,0:T(8,128)(2,1)}, u32[]{:S(2)}) copy-start(bf16[256,2048]{1,0:T(8,128)(2,1)} %param.31) | copy-start | bytes 3145732
  7.2 11.2 %copy-start.2 = (bf16[32,2048]{1,0:T(8,128)(2,1)S(1)}, bf16[32,2048]{1,0:T(8,128)(2,1)}, u32[]{:S(2)}) copy-start(bf16[32,2048]{1,0:T(8,128)(2,1)} %param.22) | copy-start | bytes 393220
  7.2 10.3 %copy-start.6 = (f32[32,2,128]{2,1,0:T(2,128)S(1)}, f32[32,2,128]{2,1,0:T(2,128)}, u32[]{:S(2)}) copy-start(f32[32,2,128]{2,1,0:T(2,128)} %param.33) | copy-start | bytes 98308
  7.2 11.2 %copy-start.3 = (bf16[2048,256]{1,0:T(8,128)(2,1)S(1)}, bf16[2048,256]{1,0:T(8,128)(2,1)}, u32[]{:S(2)}) copy-start(bf16[2048,256]{1,0:T(8,128)(2,1)} %param.27) | copy-start | bytes 3145732
  7.2 41.5 %reduce-scatter.4.cloned.1.call-start = ((), (), s32[]{:S(2)}) async-start(), calls=%async_computation.5 | async-start | bytes 163840 | tf_op jit(solution)/shard_map/reduce_scatter | solution.py:83
  13.9 8.5 %copy-start.7 = (f32[32,2]{0,1:T(2,128)}, f32[32,2]{0,1:T(2,128)S(1)}, u32[]{:S(2)}) copy-start(f32[32,2]{0,1:T(2,128)S(1)} %get-tuple-element.22) | copy-start | bytes 772
  22.4 2.0 copy-start.1
  24.5 1.7 copy-start.9
  24.5 63.0 %copy-start.4 = (bf16[512,704]{0,1:T(8,128)(2,1)S(1)}, bf16[512,704]{0,1:T(8,128)(2,1)}, u32[]{:S(2)}) copy-start(bf16[512,704]{0,1:T(8,128)(2,1)} %param.41) | copy-start | bytes 2162692
  24.5 63.4 %copy-start.5 = (bf16[512,704]{0,1:T(8,128)(2,1)S(1)}, bf16[512,704]{0,1:T(8,128)(2,1)}, u32[]{:S(2)}) copy-start(bf16[512,704]{0,1:T(8,128)(2,1)} %param.40) | copy-start | bytes 2162692
  89.2 12.6 %all-to-all-start = ((bf16[8,16,512]{2,1,0:T(8,128)(2,1)}), bf16[8,16,512]{2,1,0:T(8,128)(2,1)S(1)}, u32[]{:S(2)}, u32[]{:S(2)}) async-start(bf16[8,16,512]{2,1,0:T(8,128)(2,1)} %bitcast.6), calls=%async_computation.1 | async-start | bytes 262144 | tf_op jit(solution)/shard_map/all_to_all | solution.py:145
  94.5 38.1 %all-reduce.3.cloned.1.call-start = ((), (), s32[]{:S(2)}) async-start(), calls=%async_computation.7 | async-start | bytes 1441792 | tf_op jit(solution)/shard_map/psum | solution.py:118
  95.5 61.3 %reduce-scatter.6.cloned.1.call-start = ((), (), s32[]{:S(2)}) async-start(), calls=%async_computation.6 | async-start | bytes 655360 | tf_op jit(solution)/shard_map/reduce_scatter | solution.py:152
  113.8 19.9 %copy-start.10 = (bf16[704,512]{1,0:T(8,128)(2,1)S(1)}, bf16[704,512]{1,0:T(8,128)(2,1)}, u32[]{:S(2)}) copy-start(bf16[704,512]{1,0:T(8,128)(2,1)} %param.42) | copy-start | bytes 2162692
  119.3 43.0 %copy-start.8 = (f32[32,2]{0,1:T(2,128)S(1)}, f32[32,2]{0,1:T(2,128)}, u32[]{:S(2)}) copy-start(f32[32,2]{0,1:T(2,128)} %param.36) | copy-start | bytes 772
  119.3 103.0 %reduce-scatter.8.cloned.1.call-start = ((), (), s32[]{:S(2)}) async-start(), calls=%async_computation.8 | async-start | bytes 294912 | tf_op jit(solution)/shard_map/reduce_scatter | solution.py:121
  156.7 12.9 %all-to-all-start.1 = ((bf16[8,16,512]{2,1,0:T(8,128)(2,1)}), bf16[8,16,512]{2,1,0:T(8,128)(2,1)S(1)}, u32[]{:S(2)}, u32[]{:S(2)}) async-start(bf16[8,16,512]{2,1,0:T(8,128)(2,1)} %bitcast.62), calls=%async_computation.3 | async-start | bytes 262144 | tf_op jit(solution)/shard_map/all_to_all | solution.py:155
Sparse Core Ops, SparseCore 0:
  26.3 22.3 reduce-scatter.3
  97.7 34.8 all-reduce.2
  135.0 21.6 reduce-scatter.5
  159.9 62.4 reduce-scatter.7
where the time goes:
time: 238 us; the launch traced here: 237 us
  waiting for transfers between devices  121 us (51%)
  blocking collectives  51.8 us (22%)
  matrix products  20.2 us (8%)
  between operations  14.1 us (6%)
  other arithmetic  13.3 us (6%)
  starting transfers between devices  11 us (5%)
  local copies, waits for them, and re-layouts  5.31 us (2%)
    reduce_scatter x1, waiting for transfers between devices, local(): lax.psum_scatter(jnp.dot(dense_hidden, dense_down, preferred_element_type...  52.6 us
    all_gather x1, blocking collectives, local(): rows_in = lax.all_gather(normed, 'ep', axis=0, tiled=True)  31.2 us
    reduce_scatter x1, waiting for transfers between devices, local(): lax.psum_scatter(partial_out.astype(jnp.bfloat16), 'tp', scatter_dimensio...  21.8 us
    reduce_scatter x1, waiting for transfers between devices, local(): lax.psum_scatter(branch_terms.astype(jnp.bfloat16), 'tp', scatter_dimensi...  20.2 us
    psum x1, waiting for transfers between devices, local(): lax.psum(dense_pre.astype(jnp.bfloat16), 'tp').astype(jnp.float32)  13.2 us
    all_gather x1, blocking collectives, local(): full_rows = lax.all_gather(arrived, 'tp', axis=2, tiled=True)  9.21 us
    all_to_all x1, waiting for transfers between devices, local(): lax.all_to_all(summed_out.reshape(arrived.shape), 'ep', split_axis=0, con...  7.21 us
    all_to_all x1, waiting for transfers between devices, local(): lax.all_to_all(outgoing, 'ep', split_axis=0, concat_axis=0, tiled=True)  6.31 us
  transfers between devices with their start and end apart: 6, of which 6 were waited for; matrix products, arithmetic and copies ran while one was open for 6% of the time, Pallas kernels for 0%

commit v1 on v0

--- a/solution.py
+++ b/solution.py
@@ -115,7 +115,9 @@
         ],
         axis=1,
     )
-    dense_pre = lax.psum(dense_pre.astype(jnp.bfloat16), "tp").astype(jnp.float32)
+    dense_pre = jnp.sum(lax.all_gather(dense_pre.astype(jnp.bfloat16), "tp"), axis=0).astype(
+        jnp.float32
+    )
     dense_pre_gate, dense_pre_up = jnp.split(dense_pre, 2, axis=1)
     dense_hidden = (jax.nn.silu(dense_pre_gate) * dense_pre_up).astype(jnp.bfloat16)
     dense_out = lax.psum_scatter(

time: 238 us -> 224 us (0.941)
  waiting for transfers between devices: 121 us -> 104 us
  blocking collectives: 51.8 us -> 61.7 us
  starting transfers between devices: 11 us -> 3.55 us
    reduce_scatter x1, waiting for transfers between devices: 21.8 us -> 0.02 us  [local(): lax.psum_scatter(partial_out.astype(jnp.bfloat16), 'tp', scatter_dimensio...]
    all_gather x0 -> x1, waiting for transfers between devices: none -> 21 us  [local(): lax.all_gather(dense_pre.astype(jnp.bfloat16), 'tp')]
    psum x1 -> x0, waiting for transfers between devices: 13.2 us -> none  [local(): lax.psum(dense_pre.astype(jnp.bfloat16), 'tp').astype(jnp.float32)]
    all_to_all x0 -> x1, blocking collectives: none -> 12.8 us  [local(): lax.all_to_all(outgoing, 'ep', split_axis=0, concat_axis=0, tiled=True)]
    reduce_scatter x1, waiting for transfers between devices: 52.6 us -> 62.3 us  [local(): lax.psum_scatter(jnp.dot(dense_hidden, dense_down, preferred_element_type...]
    all_to_all x1, waiting for transfers between devices: 7.21 us -> 0.01 us  [local(): lax.all_to_all(summed_out.reshape(arrived.shape), 'ep', split_axis=0, con...]
    all_to_all x1 -> x0, waiting for transfers between devices: 6.31 us -> none  [local(): lax.all_to_all(outgoing, 'ep', split_axis=0, concat_axis=0, tiled=True)]
    all_to_all x1 -> x0, starting transfers between devices: 5.3 us -> none  [local(): lax.all_to_all(outgoing, 'ep', split_axis=0, concat_axis=0, tiled=True)]
  transfers between devices with their start and end apart: 6 -> 5, of which waited for: 6 -> 3; matrix products, arithmetic and copies ran while one was open for 6% -> 4% of each run, Pallas kernels for 0% -> 0%
where the time goes in v1:
time: 224 us; the launch traced here: 223 us
  waiting for transfers between devices  104 us (46%)
  blocking collectives  61.7 us (28%)
  matrix products  19.4 us (9%)
  between operations  14.1 us (6%)
  other arithmetic  13.9 us (6%)
  local copies, waits for them, and re-layouts  6.73 us (3%)
  starting transfers between devices  3.55 us (2%)
    reduce_scatter x1, waiting for transfers between devices, local(): lax.psum_scatter(jnp.dot(dense_hidden, dense_down, preferred_element_type...  62.3 us
    all_gather x1, blocking collectives, local(): rows_in = lax.all_gather(normed, 'ep', axis=0, tiled=True)  30.9 us
    all_gather x1, waiting for transfers between devices, local(): lax.all_gather(dense_pre.astype(jnp.bfloat16), 'tp')  21 us
    reduce_scatter x1, waiting for transfers between devices, local(): lax.psum_scatter(branch_terms.astype(jnp.bfloat16), 'tp', scatter_dimensi...  20.3 us
    all_to_all x1, blocking collectives, local(): lax.all_to_all(outgoing, 'ep', split_axis=0, concat_axis=0, tiled=True)  12.8 us
    all_gather x1, blocking collectives, local(): full_rows = lax.all_gather(arrived, 'tp', axis=2, tiled=True)  6.49 us
    psum x1, blocking collectives, local(): lax.psum((jnp.sum(branch * branch, axis=-1), jnp.sum(start_part * start_p...  5.77 us
    psum x1, blocking collectives, local(): ffn_sq = lax.psum(jnp.sum(ffn * ffn, axis=-1), 'tp')  5.66 us
  transfers between devices with their start and end apart: 5, of which 3 were waited for; matrix products, arithmetic and copies ran while one was open for 4% of the time, Pallas kernels for 0%

profile of v1, /device:TPU:0, one launch (start us, length us, event | category | flops | bytes accessed | tf_op | source)
XLA Modules:
  0.0 222.9 jit_solution(11885395427747576943)
XLA Ops:
  7.3 0.9 slice.14
  8.2 1.0 multiply_reduce_fusion
  9.2 1.6 convolution_convert_fusion.7
  10.9 1.1 fusion.46
  12.0 0.7 dynamic_slice.21
  12.8 1.2 subtract_exponential_fusion
  14.1 1.6 convolution_convert_fusion.6
  15.8 1.6 convolution_convert_fusion.5
  17.5 0.8 fusion.40
  18.7 3.7 %multiply_add_fusion = f32[32,2,128,128]{3,2,1,0:T(8,128)S(1)} fusion(f32[32,2,128,128]{3,2,1,0:T(8,128)} %param.32, f32[32,2,128]{2,1,0:T(2,128)S(1)} %reshape.143, f32[32,2,128]{2,1,0:T(2,128)S(1)} %get-tuple-element.20, f32[32,2]{1,0:T(8,128)S(1)} %copy.37), kind=kLoop, calls=%fused_computation | loop fusion | flops 3145728 | bytes 8454400 | tf_op jit(solution)/shard_map/add | solution.py:72
  22.5 2.0 copy-done.1
  25.2 0.9 convolution_convert_fusion
  26.8 0.9 fusion.58
  27.7 0.8 dynamic-slice_multiply_fusion
  28.5 20.3 %reduce-scatter.4.cloned.1.call-done = bf16[32,512]{1,0:T(8,128)(2,1)} async-done(((bf16[32,2048]{1,0:T(8,128)(2,1)}), bf16[32,512]{1,0:T(8,128)(2,1)}) %reduce-scatter.4.cloned.1.call-update) | async-done | bytes 32784 | tf_op jit(solution)/shard_map/reduce_scatter | solution.py:83
  48.8 1.0 multiply_reduce_fusion.2
  49.7 5.8 %all-reduce = (f32[32]{0:T(128)S(1)}, f32[32]{0:T(128)S(1)}, f32[32]{0:T(128)S(1)}, f32[32]{0:T(128)S(1)}, f32[32]{0:T(128)S(1)}, /*index=5*/f32[32]{0:T(128)S(1)}) all-reduce(f32[32]{0:T(128)S(1)} %get-tuple-element.9, f32[32]{0:T(128)S(1)} %get-tuple-element.8, f32[32]{0:T(128)S(1)} %get-tuple-element.5, ...), channel_id=1, replica_groups=mesh['ep'=8,'tp'=4] {'tp'}, use_global_device_ids=true, to_apply=%region_3.4 | all-reduce | flops 192 | bytes 1536 | tf_op jit(solution)/shard_map/psum | solution.py:91
  55.5 0.9 multiply_convert_fusion.1
  56.6 12.8 %all_to_all.10 = bf16[8,16,512]{2,1,0:T(8,128)(2,1)S(1)} all-to-all(bf16[8,16,512]{2,1,0:T(8,128)(2,1)S(1)} %bitcast.58), channel_id=1, replica_groups=mesh['ep'=8,'tp'=4] {'ep'}, dimensions={0} | all-to-all | bytes 262144 | tf_op jit(solution)/shard_map/all_to_all | solution.py:147
  69.4 6.5 %all_gather.10 = bf16[8,16,2048]{2,1,0:T(8,128)(2,1)S(1)} all-gather(bf16[8,16,512]{2,1,0:T(8,128)(2,1)S(1)} %all_to_all.10), channel_id=1, replica_groups=mesh['ep'=8,'tp'=4] {'tp'}, dimensions={2}, use_global_device_ids=true | all-gather | bytes 655360 | tf_op jit(solution)/shard_map/all_gather | solution.py:148
  75.9 2.8 %fusion.4 = f32[128,896]{1,0:T(8,128)S(1)} fusion(bf16[128,2048]{1,0:T(8,128)(2,1)S(1)} %bitcast.55, bf16[1,2048,896]{2,1,0:T(8,128)(2,1)} %param.37), kind=kOutput, calls=%fused_computation.5 | convolution fusion | flops 469762048 | bytes 4653056 | tf_op jit(solution)/shard_map/dot_general | solution.py:150
  78.7 5.4 %fusion.6 = bf16[128,2048]{1,0:T(8,128)(2,1)} fusion(bf16[1,896,2048]{2,1,0:T(8,128)(2,1)} %param.39, bf16[128,2048]{1,0:T(8,128)(2,1)S(1)} %bitcast.56, bf16[1,2048,896]{2,1,0:T(8,128)(2,1)} %param.38, f32[128,896]{1,0:T(8,128)S(1)} %fusion.4), kind=kOutput, calls=%fused_computation.7 | convolution fusion | flops 940474368 | bytes 8847360 | tf_op jit(solution)/shard_map/dot_general | solution.py:153
  84.1 30.9 %all_gather.11 = bf16[256,512]{1,0:T(8,128)(2,1)S(1)} all-gather(bf16[32,512]{1,0:T(8,128)(2,1)S(1)} %get-tuple-element.23), channel_id=1, replica_groups=mesh['ep'=8,'tp'=4] {'ep'}, dimensions={0}, use_global_device_ids=true | all-gather | bytes 294912 | tf_op jit(solution)/shard_map/all_gather | solution.py:110
  115.9 1.1 copy.43
  117.1 3.4 %all-to-all-start.1 = ((bf16[8,16,512]{2,1,0:T(8,128)(2,1)}), bf16[8,16,512]{2,1,0:T(8,128)(2,1)S(1)}, u32[]{:S(2)}, u32[]{:S(2)}) async-start(bf16[8,16,512]{2,1,0:T(8,128)(2,1)} %bitcast.67), calls=%async_computation.3 | async-start | bytes 262144 | tf_op jit(solution)/shard_map/all_to_all | solution.py:157
  120.6 21.0 %all-gather.2.cloned.1.call-done = bf16[4,256,1408]{2,1,0:T(8,128)(2,1)} async-done(((bf16[1,256,1408]{2,1,0:T(8,128)(2,1)}), bf16[4,256,1408]{2,1,0:T(8,128)(2,1)}) %all-gather.2.cloned.1.call-update) | async-done | bytes 2883600 | tf_op jit(solution)/shard_map/all_gather | solution.py:118
  141.6 2.6 %reduce_sum.121 = bf16[256,1408]{1,0:T(8,128)(2,1)S(1)} reduce(bf16[4,256,1408]{2,1,0:T(8,128)(2,1)} %all-gather.2.cloned.1.call-done, bf16[]{:T(256)} %constant.50.clone.1), dimensions={0}, to_apply=%region_19.20 | reduce | flops 1081344 | bytes 3604482 | tf_op jit(solution)/shard_map/reduce_sum | solution.py:118
  144.6 1.1 convolution_convert_fusion.3
  146.0 62.3 %reduce-scatter.8.cloned.1.call-done = bf16[32,512]{1,0:T(8,128)(2,1)} async-done(((bf16[256,512]{1,0:T(8,128)(2,1)}), bf16[32,512]{1,0:T(8,128)(2,1)}) %reduce-scatter.8.cloned.1.call-update) | async-done | bytes 32784 | tf_op jit(solution)/shard_map/reduce_scatter | solution.py:123
  208.3 0.9 multiply_reduce_fusion.1
  209.3 5.7 %psum.55 = f32[32]{0:T(128)S(1)} all-reduce(f32[32]{0:T(128)S(1)} %multiply_reduce_fusion.1), channel_id=1, replica_groups=mesh['ep'=8,'tp'=4] {'tp'}, use_global_device_ids=true, to_apply=%region_22.23 | all-reduce | flops 32 | bytes 256 | tf_op jit(solution)/shard_map/psum | solution.py:171
  214.9 1.5 add_convert_fusion
  (67 shorter events, 4.1 us)
Async XLA Ops:
  7.2 18.1 %copy-start = (bf16[256,2048]{1,0:T(8,128)(2,1)S(1)}, bf16[256,2048]{1,0:T(8,128)(2,1)}, u32[]{:S(2)}) copy-start(bf16[256,2048]{1,0:T(8,128)(2,1)} %param.31) | copy-start | bytes 3145732
  7.2 11.2 %copy-start.2 = (bf16[32,2048]{1,0:T(8,128)(2,1)S(1)}, bf16[32,2048]{1,0:T(8,128)(2,1)}, u32[]{:S(2)}) copy-start(bf16[32,2048]{1,0:T(8,128)(2,1)} %param.22) | copy-start | bytes 393220
  7.2 10.3 %copy-start.6 = (f32[32,2,128]{2,1,0:T(2,128)S(1)}, f32[32,2,128]{2,1,0:T(2,128)}, u32[]{:S(2)}) copy-start(f32[32,2,128]{2,1,0:T(2,128)} %param.33) | copy-start | bytes 98308
  7.2 11.2 %copy-start.3 = (bf16[2048,256]{1,0:T(8,128)(2,1)S(1)}, bf16[2048,256]{1,0:T(8,128)(2,1)}, u32[]{:S(2)}) copy-start(bf16[2048,256]{1,0:T(8,128)(2,1)} %param.27) | copy-start | bytes 3145732
  7.2 41.5 %reduce-scatter.4.cloned.1.call-start = ((), (), s32[]{:S(2)}) async-start(), calls=%async_computation.5 | async-start | bytes 163840 | tf_op jit(solution)/shard_map/reduce_scatter | solution.py:83
  13.9 8.5 %copy-start.7 = (f32[32,2]{0,1:T(2,128)}, f32[32,2]{0,1:T(2,128)S(1)}, u32[]{:S(2)}) copy-start(f32[32,2]{0,1:T(2,128)S(1)} %get-tuple-element.22) | copy-start | bytes 772
  22.5 2.0 copy-start.1
  24.5 1.8 copy-start.9
  26.2 90.9 %reduce-scatter.6.cloned.1.call-start = ((), (), s32[]{:S(2)}) async-start(), calls=%async_computation.6 | async-start | bytes 655360 | tf_op jit(solution)/shard_map/reduce_scatter | solution.py:154
  78.7 36.4 %copy-start.4 = (bf16[512,704]{0,1:T(8,128)(2,1)S(1)}, bf16[512,704]{0,1:T(8,128)(2,1)}, u32[]{:S(2)}) copy-start(bf16[512,704]{0,1:T(8,128)(2,1)} %param.40) | copy-start | bytes 2162692
  78.7 36.8 %copy-start.5 = (bf16[512,704]{0,1:T(8,128)(2,1)S(1)}, bf16[512,704]{0,1:T(8,128)(2,1)}, u32[]{:S(2)}) copy-start(bf16[512,704]{0,1:T(8,128)(2,1)} %param.41) | copy-start | bytes 2162692
  84.1 57.5 %all-gather.2.cloned.1.call-start = ((), (), s32[]{:S(2)}) async-start(), calls=%async_computation.7 | async-start | bytes 3604480 | tf_op jit(solution)/shard_map/all_gather | solution.py:118
  117.1 28.7 %all-to-all-start.1 = ((bf16[8,16,512]{2,1,0:T(8,128)(2,1)}), bf16[8,16,512]{2,1,0:T(8,128)(2,1)S(1)}, u32[]{:S(2)}, u32[]{:S(2)}) async-start(bf16[8,16,512]{2,1,0:T(8,128)(2,1)} %bitcast.67), calls=%async_computation.3 | async-start | bytes 262144 | tf_op jit(solution)/shard_map/all_to_all | solution.py:157
  120.5 24.1 %copy-start.10 = (bf16[704,512]{1,0:T(8,128)(2,1)S(1)}, bf16[704,512]{1,0:T(8,128)(2,1)}, u32[]{:S(2)}) copy-start(bf16[704,512]{1,0:T(8,128)(2,1)} %param.42) | copy-start | bytes 2162692
  120.5 87.8 %reduce-scatter.8.cloned.1.call-start = ((), (), s32[]{:S(2)}) async-start(), calls=%async_computation.8 | async-start | bytes 294912 | tf_op jit(solution)/shard_map/reduce_scatter | solution.py:123
  144.4 1.4 copy-start.8
Sparse Core Ops, SparseCore 0:
  26.3 22.4 reduce-scatter.3
  84.2 19.1 reduce-scatter.5
  117.2 24.3 all-gather.1
  145.8 62.4 reduce-scatter.7
